TPU v7x, 512 devices: a whole 4x4x16 slice. The times are simulated.
512 devices in a mesh: ep: 32 (over z, core), tp: 16 (over y, x).
Axes of the slice: x: 4, y: 4, z: 16, core: 2. Of those that a mesh axis runs over, the one named last changes fastest.
Arguments:
- queries: bfloat16 [8192, 2048], P('ep', 'tp'), may hold values from -6 to 6
- key_rows: bfloat16 [8192, 1024], P('ep', 'tp'), may hold values from -6 to 6
- values: bfloat16 [8192, 1024], P('ep', 'tp'), may hold values from -140 to 140
- query_gain: float32 [64], replicated, may hold values from 0.55 to 7.5
- key_gain: float32 [64], replicated, may hold values from 0.55 to 7.5
- mix_gain: float32 [2048], replicated, may hold values from 0.1 to 1.9
- out_weight: bfloat16 [2048, 4096], P(None, 'tp'), may hold values from -0.125 to 0.125
- expert_input: bfloat16 [8192, 4096], P('ep', 'tp'), may hold values from -140 to 140
- expert_gain: float32 [4096], replicated, may hold values from 0.1 to 1.9
- route_ids: int32 [8192, 2], P('ep'), may hold values from 0 to 31, as said below
- route_weights: float32 [8192, 2], P('ep'), may hold values from 0.3 to 1.7
- expert_gate: bfloat16 [32, 4096, 2048], P('ep', None, 'tp'), may hold values from -0.09375 to 0.09375
- expert_up: bfloat16 [32, 4096, 2048], P('ep', None, 'tp'), may hold values from -0.09375 to 0.09375
- expert_down: bfloat16 [32, 2048, 4096], P('ep', None, 'tp'), may hold values from -0.125 to 0.125
Outputs:
- attended: bfloat16 [8192, 4096], P('ep', 'tp')
- expert_mix: bfloat16 [8192, 4096], P('ep', 'tp')
Inputs may be any that keep to these rules, and one draw needn't show every extreme that they name: `route_ids`: the 2 experts of a row differ. In every aligned block of 256 rows no expert is named more than 22 times, and one expert, the same for all blocks, is named exactly 22 times in every block.
All inputs are finite; a program needn't handle non-finite values.
Results may differ from a plain program's by a relative error of at most 0.01.
The roundings to bfloat16 on the way count: a program that leaves them out, or rounds other values in their place, can miss the bound.
Values may be sent and summed in bfloat16 or wider, within the bound.
A program may use at most 64 MiB of HBM per device.

v0:
```python
import math
import jax
import jax.numpy as jnp
from jax import lax
from jax.sharding import Mesh
from jax.sharding import PartitionSpec as P

Q_HEADS = 32
KV_HEADS = 16
HEAD = 64
GRID_W = 64
EP = ("ep_0", "ep_1")
EPS = 1e-06
THETA = 10000.0


def in_one_piece(arrays, axis, dim, along):
    widths = [a.shape[along] for a in arrays]
    both = jnp.concatenate(arrays, axis=along)
    filled = lax.all_gather(both, axis, axis=dim, tiled=True)
    return tuple(jnp.split(filled, [sum(widths[:k]) for k in range(1, len(widths))], axis=along))


def split_up(array, dim, length):
    before, after = (array.shape[:dim], array.shape[dim + 1 :])
    return jnp.moveaxis(array.reshape(*before, length, -1, *after), dim, 0)


def joined_along(blocks, dim):
    lengths = list(blocks.shape[1:])
    lengths[dim] *= blocks.shape[0]
    return jnp.moveaxis(blocks, 0, dim).reshape(lengths)


def exchange_in_order(blocks, axes, order):
    inside = blocks.shape[1:]
    filled = blocks.reshape(*(lax.axis_size(a) for a in axes), *inside)
    for k in order:
        filled = lax.all_to_all(filled, axes[k], k, k, tiled=True)
    return filled.reshape(-1, *inside)


def exchange_by_chip(array, groups, order, split_dim, concat_dim):
    length = lax.axis_size(groups[0]) * lax.axis_size(groups[1])
    blocks = split_up(array, split_dim, length)
    return joined_along(exchange_in_order(blocks, groups, order), concat_dim)


def turn_tables(offset, length):
    half_width = HEAD // 2
    inverse = THETA ** (-jnp.arange(0, half_width, 2, dtype=jnp.float32) / half_width)
    positions = offset + jnp.arange(length, dtype=jnp.int32)
    grid_rows = (positions // GRID_W).astype(jnp.float32)
    grid_cols = (positions % GRID_W).astype(jnp.float32)
    angles = jnp.concatenate([grid_rows[:, None] * inverse, grid_cols[:, None] * inverse], axis=-1)
    return (jnp.cos(angles), jnp.sin(angles))


def norm_turn(source, scale_gain, cosine_table, sine_table):
    length = source.shape[0]
    head_rows = source.astype(jnp.float32).reshape(length, -1, HEAD)
    head_rows = (
        head_rows
        * lax.rsqrt(jnp.mean(head_rows * head_rows, axis=-1, keepdims=True) + EPS)
        * scale_gain
    )
    pair_view = head_rows.reshape(length, head_rows.shape[1], HEAD // 2, 2)
    even_part = pair_view[..., 0]
    odd_part = pair_view[..., 1]
    cosine_part = cosine_table[:, None, :]
    sine_part = sine_table[:, None, :]
    turned = jnp.stack(
        [
            even_part * cosine_part - odd_part * sine_part,
            even_part * sine_part + odd_part * cosine_part,
        ],
        axis=-1,
    )
    return turned.reshape(length, -1).astype(jnp.bfloat16)


def shards(
    queries,
    key_rows,
    values,
    query_gain,
    key_gain,
    mix_gain,
    out_weight,
    expert_input,
    expert_gain,
    route_ids,
    route_weights,
    expert_gate,
    expert_up,
    expert_down,
):
    length = queries.shape[0]
    experts_count = lax.axis_size(EP)
    offset = lax.axis_index(EP) * length
    cosine_table, sine_table = turn_tables(offset, length)
    query_turned = norm_turn(queries, query_gain, cosine_table, sine_table)
    key_turned = norm_turn(key_rows, key_gain, cosine_table, sine_table)
    kv_local = key_rows.shape[1] // HEAD
    group_size = Q_HEADS // KV_HEADS
    query_heads = query_turned.reshape(length, kv_local, group_size, HEAD)
    start_state = (
        jnp.full((kv_local, group_size, length), -jnp.inf, jnp.float32),
        jnp.zeros((kv_local, group_size, length), jnp.float32),
        jnp.zeros((length, kv_local, group_size, HEAD), jnp.float32),
    )
    key_piece, value_piece = in_one_piece((key_turned, values), EP, 0, 1)
    piece_rows = key_piece.shape[0]
    step_rows = 1024
    key_blocks = key_piece.reshape(piece_rows // step_rows, step_rows, kv_local, HEAD)
    value_blocks = value_piece.reshape(piece_rows // step_rows, step_rows, kv_local, HEAD)

    def absorb(current, block_pair):
        running_max, running_sum, running_acc = current
        key_block, value_block = block_pair
        scores = jnp.einsum(
            "rhgd,nhd->hgrn", query_heads, key_block, preferred_element_type=jnp.float32
        ) / math.sqrt(HEAD)
        new_max = jnp.maximum(running_max, jnp.max(scores, axis=-1))
        factor = jnp.exp(running_max - new_max)
        raw_weights = jnp.exp(scores - new_max[..., None])
        new_sum = running_sum * factor + jnp.sum(raw_weights, axis=-1)
        rounded = raw_weights.astype(jnp.bfloat16)
        increment = jnp.einsum(
            "hgrn,nhd->rhgd", rounded, value_block, preferred_element_type=jnp.float32
        )
        new_acc = running_acc * jnp.transpose(factor, (2, 0, 1))[..., None] + increment
        return ((new_max, new_sum, new_acc), None)

    result, unused = lax.scan(absorb, start_state, (key_blocks, value_blocks))
    heads_out = (
        (result[2] / jnp.transpose(result[1], (2, 0, 1))[..., None])
        .reshape(length, -1)
        .astype(jnp.bfloat16)
    )
    top_count = route_ids.shape[1]
    copies = route_ids.shape[0] * top_count
    capacity = (4 * copies + 3 * experts_count - 1) // (3 * experts_count)
    slot_total = experts_count * capacity
    flat_ids = route_ids.reshape(copies)
    hit_marks = (flat_ids[:, None] == jnp.arange(experts_count, dtype=jnp.int32)[None, :]).astype(
        jnp.int32
    )
    earlier = jnp.cumsum(hit_marks, axis=0) - hit_marks
    places = jnp.sum(earlier * hit_marks, axis=1)
    slot_index = flat_ids * capacity + places
    slot_rows = (
        jnp.full((slot_total,), route_ids.shape[0], jnp.int32)
        .at[slot_index]
        .set(jnp.arange(copies, dtype=jnp.int32) // top_count)
    )
    width_local = expert_input.shape[1]
    padded = jnp.concatenate([expert_input, jnp.zeros((1, width_local), jnp.bfloat16)], axis=0)
    outgoing = padded[slot_rows].reshape(experts_count, capacity, width_local)
    arrived = exchange_by_chip(outgoing, ("ep_0", "ep_1"), (1, 0), 0, 0).reshape(
        slot_total, width_local
    )
    piece_float = lax.all_gather(arrived, "tp", axis=1, tiled=True).astype(jnp.float32)
    gain_piece = expert_gain
    scaled_piece = (piece_float * gain_piece).astype(jnp.bfloat16)
    gate_rows = expert_gate[0]
    up_rows = expert_up[0]
    gate_sum = jnp.dot(scaled_piece, gate_rows, preferred_element_type=jnp.float32)
    up_sum = jnp.dot(scaled_piece, up_rows, preferred_element_type=jnp.float32)
    square_sum = jnp.sum(piece_float * piece_float, axis=1)
    row_stat = lax.rsqrt(square_sum / expert_gain.shape[0] + EPS)
    gate_value = gate_sum * row_stat[:, None]
    up_value = up_sum * row_stat[:, None]
    hidden = (jax.nn.silu(gate_value) * up_value).astype(jnp.bfloat16)
    width_out = out_weight.shape[1]
    head_piece, hidden_piece = in_one_piece((heads_out, hidden), "tp", 1, 0)
    head_float = head_piece.astype(jnp.float32)
    gain_piece = mix_gain
    mix_in = (head_float * gain_piece).astype(jnp.bfloat16)
    down_rows = expert_down[0]
    mix_sum = jnp.dot(mix_in, out_weight, preferred_element_type=jnp.float32)
    mix_squares = jnp.sum(head_float * head_float, axis=1)
    expert_sum = jnp.dot(hidden_piece, down_rows, preferred_element_type=jnp.float32)
    attended = (mix_sum * lax.rsqrt(mix_squares / mix_gain.shape[0] + EPS)[:, None]).astype(
        jnp.bfloat16
    )
    expert_back = expert_sum.astype(jnp.bfloat16).reshape(experts_count, capacity, width_out)
    returned = lax.all_to_all(expert_back, EP, split_axis=0, concat_axis=0, tiled=True).reshape(
        slot_total, width_out
    )
    picked = returned[slot_index].astype(jnp.float32) * route_weights.reshape(copies)[:, None]
    expert_mix = jnp.sum(picked.reshape(route_ids.shape[0], top_count, width_out), axis=1).astype(
        jnp.bfloat16
    )
    return (attended, expert_mix)


def solution(mesh):
    torus = Mesh(mesh.devices.reshape(16, 2, mesh.shape["tp"]), ("ep_0", "ep_1", "tp"))
    return jax.shard_map(
        shards,
        mesh=torus,
        in_specs=(
            P(EP, "tp"),
            P(EP, "tp"),
            P(EP, "tp"),
            P(),
            P(),
            P(),
            P(None, "tp"),
            P(EP, "tp"),
            P(),
            P(EP, None),
            P(EP, None),
            P(EP, None, "tp"),
            P(EP, None, "tp"),
            P(EP, None, "tp"),
        ),
        out_specs=(P(EP, "tp"), P(EP, "tp")),
        check_vma=False,
    )
```

profile of v0, /device:TPU:1, one launch (start us, length us, event | category | flops | bytes accessed | tf_op | source)
XLA Modules:
  0.0 310.1 jit_solution(1185379400146651329)
XLA Ops:
  9.4 1.4 pad_maximum_fusion.1
  15.4 2.4 scatter_custom_fusion
  17.9 2.8 gather_fusion
  20.9 10.5 %all_to_all.15 = bf16[16,2,1,22,256]{4,0,3,2,1:T(8,128)(2,1)S(1)} all-to-all(bf16[16,2,1,22,256]{4,0,3,2,1:T(8,128)(2,1)S(1)} %copy.45), channel_id=1, replica_groups=mesh['ep_0'=16,'ep_1'=2,'tp'=16] {'ep_1'}, dimensions={1} | all-to-all | bytes 720896 | tf_op jit(solution)/shard_map/all_to_all | solution.py:39
  32.5 9.6 %all-to-all-start.1 = ((bf16[16,2,1,22,256]{4,1,3,2,0:T(2,128)(2,1)}), bf16[16,2,1,22,256]{4,1,3,2,0:T(2,128)(2,1)S(1)}, u32[]{:S(2)}, u32[]{:S(2)}) async-start(bf16[16,2,1,22,256]{4,1,3,2,0:T(2,128)(2,1)} %copy.46), calls=%async_computation.1 | async-start | bytes 720896 | tf_op jit(solution)/shard_map/all_to_all | solution.py:39
  43.2 20.0 %all-to-all-done.1 = bf16[16,2,1,22,256]{4,1,3,2,0:T(2,128)(2,1)S(1)} async-done(((bf16[16,2,1,22,256]{4,1,3,2,0:T(2,128)(2,1)}), bf16[16,2,1,22,256]{4,1,3,2,0:T(2,128)(2,1)S(1)}, u32[]{:S(2)}, u32[]{:S(2)}) %all-to-all-start.1) | async-done | bytes 360480 | tf_op jit(solution)/shard_map/all_to_all | solution.py:39
  64.3 35.3 %all-gather.4.cloned.1.call-done = bf16[8192,128]{0,1:T(8,128)(2,1)} async-done(((bf16[256,128]{0,1:T(8,128)(2,1)}), bf16[8192,128]{0,1:T(8,128)(2,1)}) %all-gather.4.cloned.1.call-update) | async-done | bytes 2097168 | tf_op jit(solution)/shard_map/all_gather | solution.py:20
  99.5 1.7 fusion.70
  101.8 1.6 copy.39
  104.0 1.5 copy.40
  105.5 25.7 %while.15 = (s32[]{:T(128)}, f32[1,2,256]{2,1,0:T(2,128)S(1)}, f32[1,2,256]{2,1,0:T(2,128)S(1)}, f32[256,1,2,64]{0,3,2,1:T(8,128)S(1)}, bf16[8,1024,1,64]{1,3,2,...) while((s32[]{:T(128)}, f32[1,2,256]{2,1,0:T(2,128)S(1)}, ...), condition=%wide.region_5.6_spmd.clone, body=%wide.region_2.5_spmd.clone.sunk | while | flops 138513408 | bytes 6914169 | solution.py:135
  107.3 1.4 fusion.82
  110.5 1.4 fusion.82
  111.9 1.4 bitcast_reduce_fusion.3
  113.7 1.4 fusion.82
  117.0 1.4 fusion.82
  120.2 1.4 fusion.82
  123.4 1.4 fusion.82
  124.8 1.4 bitcast_reduce_fusion.3
  126.6 1.4 fusion.82
  129.8 1.4 fusion.82
  131.4 42.5 %all-gather.6.cloned.1.call-done = bf16[704,4096]{1,0:T(8,128)(2,1)} async-done(((bf16[704,256]{1,0:T(8,128)(2,1)}), bf16[704,4096]{1,0:T(8,128)(2,1)}) %all-gather.6.cloned.1.call-update) | async-done | bytes 5767184 | tf_op jit(solution)/shard_map/all_gather | solution.py:163
  173.9 4.0 %fusion.19 = f32[704]{0:T(1024)S(1)} fusion(bf16[704,4096]{1,0:T(8,128)(2,1)} %all-gather.6.cloned.1.call-done), kind=kLoop, calls=%fused_computation.32 | loop fusion | flops 8650048 | bytes 5769984 | tf_op jit(solution)/shard_map/reduce_sum | solution.py:170
  178.2 3.0 fusion.31
  181.2 1.7 fusion.40
  183.7 70.5 %all-gather.8.cloned.1.call-done = bf16[960,2048]{1,0:T(8,128)(2,1)} async-done(((bf16[960,128]{1,0:T(8,128)(2,1)}), bf16[960,2048]{1,0:T(8,128)(2,1)}) %all-gather.8.cloned.1.call-update) | async-done | bytes 3932176 | tf_op jit(solution)/shard_map/all_gather | solution.py:20
  254.2 2.7 fusion.28
  257.8 14.4 %all-to-all-start.2 = ((bf16[32,22,256]{2,1,0:T(8,128)(2,1)}), bf16[32,22,256]{2,1,0:T(8,128)(2,1)S(1)}, u32[]{:S(2)}, u32[]{:S(2)}) async-start(bf16[32,22,256]{2,1,0:T(8,128)(2,1)} %reshape.435), calls=%async_computation.2 | async-start | bytes 786432 | tf_op jit(solution)/shard_map/all_to_all | solution.py:188
  272.3 1.5 fusion.27
  273.8 2.3 fusion.43
  276.2 23.7 %all-to-all-done.2 = bf16[32,22,256]{2,1,0:T(8,128)(2,1)S(1)} async-done(((bf16[32,22,256]{2,1,0:T(8,128)(2,1)}), bf16[32,22,256]{2,1,0:T(8,128)(2,1)S(1)}, u32[]{:S(2)}, u32[]{:S(2)}) %all-to-all-start.2) | async-done | bytes 360480 | tf_op jit(solution)/shard_map/all_to_all | solution.py:188
  300.0 2.0 gather_fusion.1
  (122 shorter events, 26.7 us)
Async XLA Ops:
  7.2 247.0 %copy-start = (bf16[1,2048,256]{2,1,0:T(8,128)(2,1)S(1)}, bf16[1,2048,256]{2,1,0:T(8,128)(2,1)}, u32[]{:S(2)}) copy-start(bf16[1,2048,256]{2,1,0:T(8,128)(2,1)} %param.29) | copy-start | bytes 3145732
  7.2 92.3 %all-gather.4.cloned.1.call-start = ((), (), s32[]{:S(2)}) async-start(), calls=%async_computation.3 | async-start | bytes 2162688 | tf_op jit(solution)/shard_map/all_gather | solution.py:20
  17.9 24.3 %copy-start.2 = (bf16[256,128]{1,0:T(8,128)(2,1)S(1)}, bf16[256,128]{1,0:T(8,128)(2,1)}, u32[]{:S(2)}) copy-start(bf16[256,128]{1,0:T(8,128)(2,1)} %param.16) | copy-start | bytes 196612
  17.9 24.5 %copy-start.4 = (f32[64]{0:T(128)S(1)}, f32[64]{0:T(128)}, u32[]{:S(2)}) copy-start(f32[64]{0:T(128)} %param.19) | copy-start | bytes 772
  32.5 30.6 %all-to-all-start.1 = ((bf16[16,2,1,22,256]{4,1,3,2,0:T(2,128)(2,1)}), bf16[16,2,1,22,256]{4,1,3,2,0:T(2,128)(2,1)S(1)}, u32[]{:S(2)}, u32[]{:S(2)}) async-start(bf16[16,2,1,22,256]{4,1,3,2,0:T(2,128)(2,1)} %copy.46), calls=%async_computation.1 | async-start | bytes 720896 | tf_op jit(solution)/shard_map/all_to_all | solution.py:39
  42.1 131.8 %all-gather.6.cloned.1.call-start = ((), (), s32[]{:S(2)}) async-start(), calls=%async_computation.4 | async-start | bytes 6127616 | tf_op jit(solution)/shard_map/all_gather | solution.py:163
  64.0 190.1 %all-gather.8.cloned.1.call-start = ((), (), s32[]{:S(2)}) async-start(), calls=%async_computation.5 | async-start | bytes 4177920 | tf_op jit(solution)/shard_map/all_gather | solution.py:20
  131.2 46.7 %copy-start.7 = (f32[4096]{0:T(1024)S(1)}, f32[4096]{0:T(1024)}, u32[]{:S(2)}) copy-start(f32[4096]{0:T(1024)} %param.24) | copy-start | bytes 49156
  173.9 4.3 %copy-start.1 = (bf16[704,4096]{1,0:T(8,128)(2,1)S(1)}, bf16[704,4096]{1,0:T(8,128)(2,1)}, u32[]{:S(2)}) copy-start(bf16[704,4096]{1,0:T(8,128)(2,1)} %all-gather.6.cloned.1.call-done) | copy-start | bytes 17301508
  178.2 3.0 copy-start.5
  183.7 88.5 %copy-start.3 = (f32[256,2]{0,1:T(2,128)S(1)}, f32[256,2]{0,1:T(2,128)}, u32[]{:S(2)}) copy-start(f32[256,2]{0,1:T(2,128)} %param.26) | copy-start | bytes 6148
  183.7 90.1 %copy-start.6 = (bf16[2048,256]{1,0:T(8,128)(2,1)S(1)}, bf16[2048,256]{1,0:T(8,128)(2,1)}, u32[]{:S(2)}) copy-start(bf16[2048,256]{1,0:T(8,128)(2,1)} %param.22) | copy-start | bytes 3145732
  183.7 90.1 %copy-start.8 = (f32[2048]{0:T(1024)S(1)}, f32[2048]{0:T(1024)}, u32[]{:S(2)}) copy-start(f32[2048]{0:T(1024)} %param.21) | copy-start | bytes 24580
  257.8 42.1 %all-to-all-start.2 = ((bf16[32,22,256]{2,1,0:T(8,128)(2,1)}), bf16[32,22,256]{2,1,0:T(8,128)(2,1)S(1)}, u32[]{:S(2)}, u32[]{:S(2)}) async-start(bf16[32,22,256]{2,1,0:T(8,128)(2,1)} %reshape.435), calls=%async_computation.2 | async-start | bytes 786432 | tf_op jit(solution)/shard_map/all_to_all | solution.py:188
Sparse Core Ops, SparseCore 0:
  10.9 88.5 all-gather.3
  102.5 71.3 all-gather.5
  183.8 70.3 all-gather.7
where the time goes:
time: 311 us; the launch traced here: 310 us
  waiting for transfers between devices  192 us (62%)
  matrix products  31.9 us (10%)
  starting transfers between devices  24.3 us (8%)
  local copies, waits for them, and re-layouts  20.2 us (6%)
  other arithmetic  16.7 us (5%)
  between operations  14.2 us (5%)
  blocking collectives  10.5 us (3%)
    all_gather x2, waiting for transfers between devices, in_one_piece(): filled = lax.all_gather(both, axis, axis=dim, tiled=True)  106 us
    all_gather x1, waiting for transfers between devices, shards(): lax.all_gather(arrived, 'tp', axis=1, tiled=True).astype(jnp.float32)  42.5 us
    all_to_all x1, waiting for transfers between devices, shards(): lax.all_to_all(expert_back, EP, split_axis=0, concat_axis=0, tiled=True)  23.7 us
    all_to_all x1, waiting for transfers between devices, exchange_in_order(): filled = lax.all_to_all(filled, axes[k], k, k, tiled=True)  20 us
    all_to_all x1, starting transfers between devices, shards(): lax.all_to_all(expert_back, EP, split_axis=0, concat_axis=0, tiled=True)  14.4 us
    dot_general x8, matrix products, absorb(): jnp.einsum('hgrn,nhd->rhgd', rounded, value_block, preferred_element_type...  11.1 us
    dot_general x8, matrix products, absorb(): jnp.einsum('rhgd,nhd->hgrn', query_heads, key_block, preferred_element_ty...  11 us
    all_to_all x1, blocking collectives, exchange_in_order(): filled = lax.all_to_all(filled, axes[k], k, k, tiled=True)  10.5 us
  transfers between devices with their start and end apart: 5, of which 5 were waited for; matrix products, arithmetic and copies ran while one was open for 16% of the time, Pallas kernels for 0%

commit v1 on v0

--- a/solution.py
+++ b/solution.py
@@ -160,7 +160,9 @@
     arrived = exchange_by_chip(outgoing, ("ep_0", "ep_1"), (1, 0), 0, 0).reshape(
         slot_total, width_local
     )
-    piece_float = lax.all_gather(arrived, "tp", axis=1, tiled=True).astype(jnp.float32)
+    piece_float = jnp.concatenate(
+        lax.all_to_all(jnp.stack([arrived] * lax.axis_size("tp")), "tp", 0, 0), axis=1
+    ).astype(jnp.float32)
     gain_piece = expert_gain
     scaled_piece = (piece_float * gain_piece).astype(jnp.bfloat16)
     gate_rows = expert_gate[0]

time: 311 us -> 295 us (0.949)
  waiting for transfers between devices: 192 us -> 166 us
  starting transfers between devices: 24.3 us -> 29.6 us
  local copies, waits for them, and re-layouts: 20.2 us -> 23.6 us
    all_gather x1 -> x0, waiting for transfers between devices: 42.5 us -> none  [shards(): lax.all_gather(arrived, 'tp', axis=1, tiled=True).astype(jnp.float32)]
    all_to_all x0 -> x1, waiting for transfers between devices: none -> 9.39 us  [shards(): lax.all_to_all(jnp.stack([arrived] * lax.axis_size('tp')), 'tp', 0, 0)]
    all_gather x2, waiting for transfers between devices: 106 us -> 113 us  [in_one_piece(): filled = lax.all_gather(both, axis, axis=dim, tiled=True)]
    all_to_all x0 -> x1, starting transfers between devices: none -> 5.37 us  [shards(): lax.all_to_all(jnp.stack([arrived] * lax.axis_size('tp')), 'tp', 0, 0)]
  transfers between devices with their start and end apart: 5 -> 5, of which waited for: 5 -> 5; matrix products, arithmetic and copies ran while one was open for 16% -> 17% of each run, Pallas kernels for 0% -> 0%
where the time goes in v1:
time: 295 us; the launch traced here: 294 us
  waiting for transfers between devices  166 us (56%)
  matrix products  30.5 us (10%)
  starting transfers between devices  29.6 us (10%)
  local copies, waits for them, and re-layouts  23.6 us (8%)
  other arithmetic  19.3 us (7%)
  between operations  14.5 us (5%)
  blocking collectives  10.5 us (4%)
    all_gather x2, waiting for transfers between devices, in_one_piece(): filled = lax.all_gather(both, axis, axis=dim, tiled=True)  113 us
    all_to_all x1, waiting for transfers between devices, shards(): lax.all_to_all(expert_back, EP, split_axis=0, concat_axis=0, tiled=True)  23.6 us
    all_to_all x1, waiting for transfers between devices, exchange_in_order(): filled = lax.all_to_all(filled, axes[k], k, k, tiled=True)  19.9 us
    all_to_all x1, starting transfers between devices, shards(): lax.all_to_all(expert_back, EP, split_axis=0, concat_axis=0, tiled=True)  14.4 us
    dot_general x8, matrix products, absorb(): jnp.einsum('hgrn,nhd->rhgd', rounded, value_block, preferred_element_type...  11.1 us
    dot_general x8, matrix products, absorb(): jnp.einsum('rhgd,nhd->hgrn', query_heads, key_block, preferred_element_ty...  11 us
    all_to_all x1, blocking collectives, exchange_in_order(): filled = lax.all_to_all(filled, axes[k], k, k, tiled=True)  10.5 us
    all_to_all x1, starting transfers between devices, exchange_in_order(): filled = lax.all_to_all(filled, axes[k], k, k, tiled=True)  9.57 us
  transfers between devices with their start and end apart: 5, of which 5 were waited for; matrix products, arithmetic and copies ran while one was open for 17% of the time, Pallas kernels for 0%

profile of v1, /device:TPU:1, one launch (start us, length us, event | category | flops | bytes accessed | tf_op | source)
XLA Modules:
  0.0 294.3 jit_solution(8911861369216282384)
XLA Ops:
  9.4 1.4 pad_maximum_fusion.1
  15.4 2.4 scatter_custom_fusion
  17.9 2.8 gather_fusion
  20.9 10.5 %all_to_all.20 = bf16[16,2,1,22,256]{4,0,3,2,1:T(8,128)(2,1)S(1)} all-to-all(bf16[16,2,1,22,256]{4,0,3,2,1:T(8,128)(2,1)S(1)} %copy.45), channel_id=1, replica_groups=mesh['ep_0'=16,'ep_1'=2,'tp'=16] {'ep_1'}, dimensions={1} | all-to-all | bytes 720896 | tf_op jit(solution)/shard_map/all_to_all | solution.py:39
  32.5 9.6 %all-to-all-start.1 = ((bf16[16,2,1,22,256]{4,1,3,2,0:T(2,128)(2,1)}), bf16[16,2,1,22,256]{4,1,3,2,0:T(2,128)(2,1)S(1)}, u32[]{:S(2)}, u32[]{:S(2)}) async-start(bf16[16,2,1,22,256]{4,1,3,2,0:T(2,128)(2,1)} %copy.46), calls=%async_computation.1 | async-start | bytes 720896 | tf_op jit(solution)/shard_map/all_to_all | solution.py:39
  43.1 19.9 %all-to-all-done.1 = bf16[16,2,1,22,256]{4,1,3,2,0:T(2,128)(2,1)S(1)} async-done(((bf16[16,2,1,22,256]{4,1,3,2,0:T(2,128)(2,1)}), bf16[16,2,1,22,256]{4,1,3,2,0:T(2,128)(2,1)S(1)}, u32[]{:S(2)}, u32[]{:S(2)}) %all-to-all-start.1) | async-done | bytes 360480 | tf_op jit(solution)/shard_map/all_to_all | solution.py:39
  63.2 3.1 %stack.17 = bf16[16,704,256]{2,1,0:T(8,128)(2,1)} broadcast(bf16[704,256]{1,0:T(8,128)(2,1)S(1)} %stack_reshape_reshape_reshape.2), dimensions={1,2} | broadcast | bytes 6127616 | tf_op jit(solution)/shard_map/stack | solution.py:164
  66.3 5.4 %all-to-all-start.2 = ((bf16[16,704,256]{2,1,0:T(8,128)(2,1)}), bf16[16,704,256]{2,1,0:T(8,128)(2,1)}, u32[]{:S(2)}, u32[]{:S(2)}) async-start(bf16[16,704,256]{2,1,0:T(8,128)(2,1)} %stack.17), calls=%async_computation.2 | async-start | bytes 11534336 | tf_op jit(solution)/shard_map/all_to_all | solution.py:164
  71.9 27.6 %all-gather.3.cloned.1.call-done = bf16[8192,128]{0,1:T(8,128)(2,1)} async-done(((bf16[256,128]{0,1:T(8,128)(2,1)}), bf16[8192,128]{0,1:T(8,128)(2,1)}) %all-gather.3.cloned.1.call-update) | async-done | bytes 2097168 | tf_op jit(solution)/shard_map/all_gather | solution.py:20
  99.5 1.7 fusion.57
  101.8 1.5 copy.39
  104.0 1.6 copy.40
  105.6 25.6 %while.15 = (s32[]{:T(128)}, f32[1,2,256]{2,1,0:T(2,128)S(1)}, f32[1,2,256]{2,1,0:T(2,128)S(1)}, f32[256,1,2,64]{0,3,2,1:T(8,128)S(1)}, bf16[8,1024,1,64]{1,3,2,...) while((s32[]{:T(128)}, f32[1,2,256]{2,1,0:T(2,128)S(1)}, ...), condition=%wide.region_5.6_spmd.clone, body=%wide.region_2.5_spmd.clone.sunk | while | flops 138513408 | bytes 6914169 | solution.py:135
  107.4 1.4 fusion.71
  110.6 1.4 fusion.71
  113.8 1.4 fusion.71
  117.0 1.4 fusion.71
  120.2 1.4 fusion.71
  123.4 1.4 fusion.71
  126.6 1.4 fusion.71
  129.8 1.4 fusion.71
  131.4 9.4 %all-to-all-done.2 = bf16[16,704,256]{2,1,0:T(8,128)(2,1)} async-done(((bf16[16,704,256]{2,1,0:T(8,128)(2,1)}), bf16[16,704,256]{2,1,0:T(8,128)(2,1)}, u32[]{:S(2)}, u32[]{:S(2)}) %all-to-all-start.2) | async-done | bytes 5767200 | tf_op jit(solution)/shard_map/all_to_all | solution.py:164
  140.8 6.5 %fusion.19 = (f32[704]{0:T(1024)S(1)}, bf16[16,88,8,256]{3,2,1,0:T(8,128)(2,1)S(1)}) fusion(bf16[16,704,256]{2,1,0:T(8,128)(2,1)} %all-to-all-done.2, f32[16,256]{1,0:T(8,128)S(1)} %mul.302), kind=kLoop, calls=%fused_computation.32 | loop fusion | flops 14417216 | bytes 11553536 | tf_op jit(solution)/shard_map/reduce_sum | solution.py:172
  148.5 1.7 convolution_multiply_fusion.1
  150.2 1.7 fusion.29
  152.7 85.4 %all-gather.5.cloned.1.call-done = bf16[960,2048]{1,0:T(8,128)(2,1)} async-done(((bf16[960,128]{1,0:T(8,128)(2,1)}), bf16[960,2048]{1,0:T(8,128)(2,1)}) %all-gather.5.cloned.1.call-update) | async-done | bytes 3932176 | tf_op jit(solution)/shard_map/all_gather | solution.py:20
  238.1 2.7 fusion.25
  241.7 14.4 %all-to-all-start.3 = ((bf16[32,22,256]{2,1,0:T(8,128)(2,1)}), bf16[32,22,256]{2,1,0:T(8,128)(2,1)S(1)}, u32[]{:S(2)}, u32[]{:S(2)}) async-start(bf16[32,22,256]{2,1,0:T(8,128)(2,1)} %reshape.450), calls=%async_computation.3 | async-start | bytes 786432 | tf_op jit(solution)/shard_map/all_to_all | solution.py:190
  256.2 1.5 fusion.24
  257.8 2.3 fusion.30
  260.1 23.6 %all-to-all-done.3 = bf16[32,22,256]{2,1,0:T(8,128)(2,1)S(1)} async-done(((bf16[32,22,256]{2,1,0:T(8,128)(2,1)}), bf16[32,22,256]{2,1,0:T(8,128)(2,1)S(1)}, u32[]{:S(2)}, u32[]{:S(2)}) %all-to-all-start.3) | async-done | bytes 360480 | tf_op jit(solution)/shard_map/all_to_all | solution.py:190
  283.9 2.0 gather_fusion.1
  (124 shorter events, 29.5 us)
Async XLA Ops:
  7.2 230.9 %copy-start = (bf16[1,2048,256]{2,1,0:T(8,128)(2,1)S(1)}, bf16[1,2048,256]{2,1,0:T(8,128)(2,1)}, u32[]{:S(2)}) copy-start(bf16[1,2048,256]{2,1,0:T(8,128)(2,1)} %param.29) | copy-start | bytes 3145732
  7.2 92.3 %all-gather.3.cloned.1.call-start = ((), (), s32[]{:S(2)}) async-start(), calls=%async_computation.4 | async-start | bytes 2162688 | tf_op jit(solution)/shard_map/all_gather | solution.py:20
  17.9 24.3 %copy-start.2 = (f32[4096]{0:T(1024)S(1)}, f32[4096]{0:T(1024)}, u32[]{:S(2)}) copy-start(f32[4096]{0:T(1024)} %param.24) | copy-start | bytes 49156
  17.9 24.3 %copy-start.1 = (bf16[256,128]{1,0:T(8,128)(2,1)S(1)}, bf16[256,128]{1,0:T(8,128)(2,1)}, u32[]{:S(2)}) copy-start(bf16[256,128]{1,0:T(8,128)(2,1)} %param.16) | copy-start | bytes 196612
  17.9 24.5 %copy-start.4 = (f32[64]{0:T(128)S(1)}, f32[64]{0:T(128)}, u32[]{:S(2)}) copy-start(f32[64]{0:T(128)} %param.19) | copy-start | bytes 772
  32.5 30.5 %all-to-all-start.1 = ((bf16[16,2,1,22,256]{4,1,3,2,0:T(2,128)(2,1)}), bf16[16,2,1,22,256]{4,1,3,2,0:T(2,128)(2,1)S(1)}, u32[]{:S(2)}, u32[]{:S(2)}) async-start(bf16[16,2,1,22,256]{4,1,3,2,0:T(2,128)(2,1)} %copy.46), calls=%async_computation.1 | async-start | bytes 720896 | tf_op jit(solution)/shard_map/all_to_all | solution.py:39
  66.3 74.5 %all-to-all-start.2 = ((bf16[16,704,256]{2,1,0:T(8,128)(2,1)}), bf16[16,704,256]{2,1,0:T(8,128)(2,1)}, u32[]{:S(2)}, u32[]{:S(2)}) async-start(bf16[16,704,256]{2,1,0:T(8,128)(2,1)} %stack.17), calls=%async_computation.2 | async-start | bytes 11534336 | tf_op jit(solution)/shard_map/all_to_all | solution.py:164
  71.7 166.4 %all-gather.5.cloned.1.call-start = ((), (), s32[]{:S(2)}) async-start(), calls=%async_computation.5 | async-start | bytes 4177920 | tf_op jit(solution)/shard_map/all_gather | solution.py:20
  147.3 1.2 copy-start.5
  148.5 1.7 copy-start.6
  152.6 103.4 %copy-start.3 = (f32[256,2]{0,1:T(2,128)S(1)}, f32[256,2]{0,1:T(2,128)}, u32[]{:S(2)}) copy-start(f32[256,2]{0,1:T(2,128)} %param.26) | copy-start | bytes 6148
  152.6 105.1 %copy-start.7 = (bf16[2048,256]{1,0:T(8,128)(2,1)S(1)}, bf16[2048,256]{1,0:T(8,128)(2,1)}, u32[]{:S(2)}) copy-start(bf16[2048,256]{1,0:T(8,128)(2,1)} %param.22) | copy-start | bytes 3145732
  152.6 105.1 %copy-start.8 = (f32[2048]{0:T(1024)S(1)}, f32[2048]{0:T(1024)}, u32[]{:S(2)}) copy-start(f32[2048]{0:T(1024)} %param.21) | copy-start | bytes 24580
  241.7 42.1 %all-to-all-start.3 = ((bf16[32,22,256]{2,1,0:T(8,128)(2,1)}), bf16[32,22,256]{2,1,0:T(8,128)(2,1)S(1)}, u32[]{:S(2)}, u32[]{:S(2)}) async-start(bf16[32,22,256]{2,1,0:T(8,128)(2,1)} %reshape.450), calls=%async_computation.3 | async-start | bytes 786432 | tf_op jit(solution)/shard_map/all_to_all | solution.py:190
Sparse Core Ops, SparseCore 0:
  10.9 88.5 all-gather.2
  152.7 85.3 all-gather.4
